TPU v7x, 32 devices: a whole 2x2x4 slice. The times are simulated.
32 devices in a mesh: sp: 8 (over z, x), tp: 4 (over y, core).
Axes of the slice: x: 2, y: 2, z: 4, core: 2. Of those that a mesh axis runs over, the one named last changes fastest.
Arguments:
- skip_stream_input: bfloat16 [1024, 2048], P('sp'), may hold values from -16 to 16
- asking_vectors_split: bfloat16 [1024, 2048], P('sp', 'tp'), may hold values from -8 to 8
- lookup_vectors_split: bfloat16 [1024, 512], P('sp'), may hold values from -8 to 8
- content_vectors_split: bfloat16 [1024, 512], P('sp'), may hold values from -6 to 6
- asking_rms_gain: float32 [128], replicated, may hold values from 0.1 to 1.9
- lookup_rms_gain: float32 [128], replicated, may hold values from 0.1 to 1.9
- softness_per_channel: float32 [16], P('tp'), may hold values from 1.5 to 24
- mixing_exit_weights: bfloat16 [2048, 2048], P('tp'), may hold values from -0.125 to 0.125
- specialist_rms_gain: float32 [2048], replicated, may hold values from 0.1 to 1.9
- selected_dispatch_weights: float32 [1024, 2], P('sp'), may hold values from -6 to 6
- selected_specialist_ids: int32 [1024, 2], P('sp'), may hold values from 0 to 7, all different within a row; in each aligned block of 128 rows (0 to 127, 128 to 255, ...) at most 48 rows name the same one
- specialist_switch_weights: bfloat16 [8, 2048, 2048], P('sp', None, 'tp'), may hold values from -0.125 to 0.125
- specialist_widen_weights: bfloat16 [8, 2048, 2048], P('sp', None, 'tp'), may hold values from -0.125 to 0.125
- specialist_shrink_weights: bfloat16 [8, 2048, 2048], P('sp', 'tp'), may hold values from -0.125 to 0.125
Outputs:
- layer_out: bfloat16 [1024, 2048], P('sp', 'tp')
Inputs may be any that keep to these rules, and one draw needn't show every extreme that they name: `selected_specialist_ids`: each row names 2 different experts. In each aligned block of 128 rows no expert is named by more than 48 rows, a bound that some block reaches.
All inputs are finite; a program needn't handle non-finite values.
Results may differ from a plain program's by a relative error of at most 0.0085.
Values may be sent and summed in bfloat16 or wider, within the bound.
A program may use at most 64 MiB of HBM per device.

v0:
```python
import math

import jax
import jax.numpy as jnp
from jax import lax
from jax.sharding import PartitionSpec as P

CHANNEL_WIDTH = 128
GROUP = 4
GRID_W = 64


EPSILON = 1e-06
NEGATIVE = -1e30


def rotate_half(values_in, positions, full_width):
    half_width = full_width // 2
    frequency = 10000.0 ** (-jnp.arange(half_width, dtype=jnp.float32) / half_width)
    angles = positions.astype(jnp.float32)[:, None] * frequency[None, :]
    cosine = jnp.cos(angles)[:, None, :]
    sine = jnp.sin(angles)[:, None, :]
    leading = values_in[..., :half_width]
    trailing = values_in[..., half_width:]
    return jnp.concatenate(
        [leading * cosine - trailing * sine, trailing * cosine + leading * sine], axis=-1
    )


def norm_rotate(heads_in, gain_vec, positions):
    widened = heads_in.astype(jnp.float32)
    scaled = (
        widened
        * lax.rsqrt(jnp.mean(widened * widened, axis=-1, keepdims=True) + EPSILON)
        * gain_vec
    )
    half_width = scaled.shape[-1] // 2
    grid_rows = positions // GRID_W
    grid_cols = positions % GRID_W
    turned = jnp.concatenate(
        [
            rotate_half(scaled[..., :half_width], grid_rows, half_width),
            rotate_half(scaled[..., half_width:], grid_cols, half_width),
        ],
        axis=-1,
    )
    return turned.astype(jnp.bfloat16)


def shards(
    skip_stream_input,
    asking_vectors_split,
    lookup_vectors_split,
    content_vectors_split,
    asking_rms_gain,
    lookup_rms_gain,
    softness_per_channel,
    mixing_exit_weights,
    specialist_rms_gain,
    selected_dispatch_weights,
    selected_specialist_ids,
    specialist_switch_weights,
    specialist_widen_weights,
    specialist_shrink_weights,
):
    tok_count = skip_stream_input.shape[0]
    model_width = skip_stream_input.shape[1]
    heads_here = asking_vectors_split.shape[1] // CHANNEL_WIDTH
    local_key_value_heads = max(1, heads_here // GROUP)
    local_group_count = heads_here // local_key_value_heads
    tp_position = lax.axis_index("tp")
    positions = lax.axis_index("sp") * tok_count + jnp.arange(tok_count, dtype=jnp.int32)
    query_turned = norm_rotate(
        asking_vectors_split.reshape(tok_count, heads_here, CHANNEL_WIDTH),
        asking_rms_gain,
        positions,
    )
    first_head = tp_position * heads_here // GROUP
    key_cols = lax.dynamic_slice_in_dim(
        lookup_vectors_split, first_head * CHANNEL_WIDTH, local_key_value_heads * CHANNEL_WIDTH, 1
    )
    value_cols = lax.dynamic_slice_in_dim(
        content_vectors_split, first_head * CHANNEL_WIDTH, local_key_value_heads * CHANNEL_WIDTH, 1
    )
    key_turned = norm_rotate(
        key_cols.reshape(tok_count, local_key_value_heads, CHANNEL_WIDTH),
        lookup_rms_gain,
        positions,
    )
    key_turned = key_turned.reshape(tok_count, local_key_value_heads * CHANNEL_WIDTH)
    query_grouped = query_turned.reshape(
        tok_count, local_key_value_heads, local_group_count, CHANNEL_WIDTH
    ).transpose(1, 2, 0, 3)
    inverse_root_width = (softness_per_channel / math.sqrt(CHANNEL_WIDTH)).reshape(
        local_key_value_heads, local_group_count, 1, 1
    )

    def absorb(run_state, key_span, value_span):
        run_max, run_sum, run_acc = run_state
        scores = (
            jnp.einsum(
                "kgqd,nkd->kgqn", query_grouped, key_span, preferred_element_type=jnp.float32
            )
            * inverse_root_width
        )
        new_max = jnp.maximum(run_max, jnp.max(scores, axis=-1))
        factor = jnp.exp(run_max - new_max)
        exp_terms = jnp.exp(scores - new_max[..., None])
        run_sum = run_sum * factor + jnp.sum(exp_terms, axis=-1)
        run_acc = run_acc * factor[..., None] + jnp.einsum(
            "kgqn,nkd->kgqd",
            exp_terms.astype(jnp.bfloat16),
            value_span,
            preferred_element_type=jnp.float32,
        )
        return (new_max, run_sum, run_acc)

    initial = (
        jnp.full((local_key_value_heads, local_group_count, tok_count), NEGATIVE, jnp.float32),
        jnp.zeros((local_key_value_heads, local_group_count, tok_count), jnp.float32),
        jnp.zeros(
            (local_key_value_heads, local_group_count, tok_count, CHANNEL_WIDTH), jnp.float32
        ),
    )
    key_piece = lax.all_gather(key_turned, "sp", axis=0, tiled=True)
    value_piece = lax.all_gather(value_cols, "sp", axis=0, tiled=True)
    piece_len = key_piece.shape[0]
    span_len = 1024
    span_count = piece_len // span_len
    key_spans = key_piece.reshape(span_count, span_len, local_key_value_heads, CHANNEL_WIDTH)
    value_spans = value_piece.reshape(span_count, span_len, local_key_value_heads, CHANNEL_WIDTH)

    def step_span(inner_state, span_pair):
        return (absorb(inner_state, span_pair[0], span_pair[1]), None)

    result_state, unused = lax.scan(step_span, initial, (key_spans, value_spans))
    final_max, final_sum, final_acc = result_state
    attn_heads = (final_acc / final_sum[..., None]).astype(jnp.bfloat16)
    attn_flat = attn_heads.transpose(2, 0, 1, 3).reshape(tok_count, heads_here * CHANNEL_WIDTH)
    partial_sum = jnp.dot(attn_flat, mixing_exit_weights, preferred_element_type=jnp.float32)
    share_width = model_width // lax.axis_size("tp")
    first_col = tp_position * share_width
    attended = lax.psum(partial_sum.astype(jnp.bfloat16), "tp")
    mid_rows = (skip_stream_input.astype(jnp.float32) + attended.astype(jnp.float32)).astype(
        jnp.bfloat16
    )
    mid_wide = mid_rows.astype(jnp.float32)
    normed_rows = (
        mid_wide
        * lax.rsqrt(jnp.mean(mid_wide * mid_wide, axis=-1, keepdims=True) + EPSILON)
        * specialist_rms_gain
    ).astype(jnp.bfloat16)
    mid_share = lax.dynamic_slice_in_dim(mid_rows, first_col, share_width, 1)
    outgoing_rows = lax.dynamic_slice_in_dim(normed_rows, first_col, share_width, 1)
    experts_count = lax.axis_size("sp")
    top_count = selected_specialist_ids.shape[1]
    capacity = max(2, 3 * tok_count * top_count // (2 * experts_count))
    flat_ids = selected_specialist_ids.reshape(-1)
    one_hot = (flat_ids[:, None] == jnp.arange(experts_count, dtype=jnp.int32)[None, :]).astype(
        jnp.int32
    )
    earlier = jnp.cumsum(one_hot, axis=0) - one_hot
    slot_index = jnp.sum(earlier * one_hot, axis=1)
    destination = flat_ids * capacity + slot_index
    owner_rows = jnp.arange(tok_count * top_count, dtype=jnp.int32) // top_count
    slot_owner = jnp.zeros((experts_count * capacity,), jnp.int32).at[destination].set(owner_rows)
    filled = jnp.zeros((experts_count * capacity,), jnp.int32).at[destination].set(1)
    outgoing = jnp.where(
        filled[:, None] > 0, outgoing_rows[slot_owner], jnp.zeros((), jnp.bfloat16)
    )
    outgoing = outgoing.reshape(experts_count, capacity, outgoing_rows.shape[1])
    gate_local = specialist_switch_weights[0]
    up_local = specialist_widen_weights[0]
    down_local = specialist_shrink_weights[0]
    arrived = lax.all_to_all(outgoing, "sp", split_axis=0, concat_axis=0, tiled=True)
    row_count = arrived.shape[0] * arrived.shape[1]
    feature_piece = lax.all_gather(arrived, "tp", axis=2, tiled=True)
    piece_width = feature_piece.shape[2]
    flat_piece = feature_piece.reshape(row_count, piece_width)
    gate_acc = jnp.dot(flat_piece, gate_local, preferred_element_type=jnp.float32)
    up_acc = jnp.dot(flat_piece, up_local, preferred_element_type=jnp.float32)
    hidden = (jax.nn.silu(gate_acc) * up_acc).astype(jnp.bfloat16)
    expert_part = jnp.dot(hidden, down_local, preferred_element_type=jnp.float32)
    expert_part = expert_part.reshape(arrived.shape[0], arrived.shape[1], model_width)
    expert_share = lax.psum_scatter(
        expert_part.astype(jnp.bfloat16), "tp", scatter_dimension=2, tiled=True
    )
    returned = lax.all_to_all(expert_share, "sp", split_axis=0, concat_axis=0, tiled=True)
    back_flat = returned.reshape(experts_count * capacity, share_width)
    picked = back_flat[destination].reshape(tok_count, top_count, share_width).astype(jnp.float32)
    route_weights = jax.nn.softmax(selected_dispatch_weights, axis=-1)
    layer_out = mid_share.astype(jnp.float32) + jnp.sum(route_weights[..., None] * picked, axis=1)
    return layer_out.astype(jnp.bfloat16)


def solution(mesh):
    in_specs = (
        P("sp", None),
        P("sp", "tp"),
        P("sp", None),
        P("sp", None),
        P(),
        P(),
        P("tp"),
        P("tp", None),
        P(),
        P("sp", None),
        P("sp", None),
        P("sp", None, "tp"),
        P("sp", None, "tp"),
        P("sp", "tp", None),
    )
    out_specs = P("sp", "tp")
    return jax.shard_map(shards, mesh=mesh, in_specs=in_specs, out_specs=out_specs, check_vma=False)
```

profile of v0, /device:TPU:0, one launch (start us, length us, event | category | flops | bytes accessed | tf_op | source)
XLA Modules:
  0.0 204.7 jit_solution(4723165117829957611)
XLA Ops:
  6.6 0.9 constant_dynamic-slice_fusion.1
  7.7 0.7 fusion.35
  8.4 0.5 multiply_cosine_fusion.1
  9.2 28.3 %all_gather.9 = bf16[1024,128]{0,1:T(8,128)(2,1)S(1)} all-gather(bf16[128,128]{0,1:T(8,128)(2,1)S(1)} %pad_maximum_fusion), channel_id=1, replica_groups=mesh['sp'=8,'tp'=4] {'sp'}, dimensions={0}, use_global_device_ids=true | all-gather | bytes 294912 | tf_op jit(solution)/shard_map/all_gather | solution.py:125
  37.5 1.0 copy.24
  38.7 0.7 broadcast_multiply_fusion.1
  39.4 0.8 multiply_multiply_fusion
  40.5 0.6 multiply_reduce_fusion
  41.1 1.3 copy-done.1
  42.4 0.5 fusion.5
  42.9 0.8 constant_dynamic-slice_fusion
  43.8 26.8 %all_gather.10 = bf16[1024,128]{0,1:T(8,128)(2,1)S(1)} all-gather(bf16[128,128]{0,1:T(8,128)(2,1)S(1)} %copy.36), channel_id=1, replica_groups=mesh['sp'=8,'tp'=4] {'sp'}, dimensions={0}, use_global_device_ids=true | all-gather | bytes 294912 | tf_op jit(solution)/shard_map/all_gather | solution.py:126
  70.7 2.2 %fusion.14 = bf16[4,128,128]{1,2,0:T(8,128)(2,1)S(1)} fusion(f32[4,128,1024]{2,1,0:T(8,128)} %copy-done.1, f32[4,128]{1,0:T(4,128)S(1)} %broadcast_maximum_fusion, f32[4]{0:T(128)S(1)} %broadcast_multiply_fusion.1, bf16[1024,128]{0,1:T(8,128)(2,1)S(1)} %all_gather.10, f32[4,128]{1,0:T(4,128)S(1)} %get-tuple-element.44, f32[4,128]{1,0:T(4,128)S(1)} %get-tuple-element.43), kind=kOutput, calls=%fused_computation.19 | convolution fusion | flops 135987200 | bytes 2496528 | tf_op jit(solution)/shard_map/while/body/eval_jaxpr/kgqn,nkd->kgqd/dot_general | solution.py:110
  72.9 1.3 convolution_convert_fusion.1
  74.7 0.6 reduce-window.6
  75.9 1.4 scatter_custom_fusion.1
  77.3 1.4 scatter_custom_fusion
  78.8 0.8 dynamic-slice
  79.6 25.8 %all-reduce.2.cloned.1.call-done = bf16[128,2048]{1,0:T(8,128)(2,1)} async-done(((bf16[128,2048]{1,0:T(8,128)(2,1)}), bf16[128,2048]{1,0:T(8,128)(2,1)}) %all-reduce.2.cloned.1.call-update) | async-done | bytes 524304 | tf_op jit(solution)/shard_map/psum | solution.py:143
  105.4 1.3 multiply_reduce_fusion.1
  106.9 2.1 %gather_fusion = bf16[384,512]{1,0:T(8,128)(2,1)S(1)} fusion(bf16[128,512]{1,0:T(8,128)(2,1)S(1)} %fusion.19, s32[1024]{0:T(1024)S(1)} %pad_clamp_fusion.1), kind=kCustom, calls=%fused_computation | custom fusion | bytes 787968 | tf_op jit(solution)/shard_map/gather | solution.py:169
  109.1 16.5 %all_to_all.10 = bf16[8,48,512]{2,1,0:T(8,128)(2,1)} all-to-all(bf16[8,48,512]{2,1,0:T(8,128)(2,1)S(1)} %broadcast_select_fusion), channel_id=1, replica_groups=mesh['sp'=8,'tp'=4] {'sp'}, dimensions={0} | all-to-all | bytes 786432 | tf_op jit(solution)/shard_map/all_to_all | solution.py:175
  125.7 18.0 %all-gather.2.cloned.1.call-done = bf16[8,48,2048]{2,1,0:T(8,128)(2,1)} async-done(((bf16[8,48,512]{2,1,0:T(8,128)(2,1)}), bf16[8,48,2048]{2,1,0:T(8,128)(2,1)}) %all-gather.2.cloned.1.call-update) | async-done | bytes 1572880 | tf_op jit(solution)/shard_map/all_gather | solution.py:177
  143.7 3.2 %fusion.3 = f32[384,512]{1,0:T(8,128)S(1)} fusion(bf16[384,2048]{1,0:T(8,128)(2,1)} %bitcast.82, bf16[1,2048,512]{2,1,0:T(8,128)(2,1)} %param.25), kind=kOutput, calls=%fused_computation.9 | convolution fusion | flops 805306368 | bytes 4456448 | tf_op jit(solution)/shard_map/dot_general | solution.py:180
  146.9 1.0 fusion.10
  147.9 2.1 %convolution_convert_fusion = bf16[8,48,2048]{2,1,0:T(8,128)(2,1)} fusion(bf16[8,48,512]{2,1,0:T(8,128)(2,1)S(1)} %bitcast.84, bf16[1,512,2048]{2,1,0:T(8,128)(2,1)S(1)} %copy-done), kind=kOutput, calls=%fused_computation.4 | convolution fusion | flops 806092800 | bytes 4063232 | tf_op jit(solution)/shard_map/dot_general | solution.py:183
  150.1 28.1 %reduce-scatter.2.cloned.1.call-done = bf16[8,48,512]{2,1,0:T(8,128)(2,1)} async-done(((bf16[8,48,2048]{2,1,0:T(8,128)(2,1)}), bf16[8,48,512]{2,1,0:T(8,128)(2,1)}) %reduce-scatter.2.cloned.1.call-update) | async-done | bytes 393232 | tf_op jit(solution)/shard_map/reduce_scatter | solution.py:185
  178.2 5.5 %all-to-all-start.1 = ((bf16[8,48,512]{2,1,0:T(8,128)(2,1)}), bf16[8,48,512]{2,1,0:T(8,128)(2,1)S(1)}, u32[]{:S(2)}, u32[]{:S(2)}) async-start(bf16[8,48,512]{2,1,0:T(8,128)(2,1)} %reduce-scatter.2.cloned.1.call-done), calls=%async_computation.2 | async-start | bytes 786432 | tf_op jit(solution)/shard_map/all_to_all | solution.py:188
  183.9 11.4 %all-to-all-done.1 = bf16[8,48,512]{2,1,0:T(8,128)(2,1)S(1)} async-done(((bf16[8,48,512]{2,1,0:T(8,128)(2,1)}), bf16[8,48,512]{2,1,0:T(8,128)(2,1)S(1)}, u32[]{:S(2)}, u32[]{:S(2)}) %all-to-all-start.1) | async-done | bytes 393248 | tf_op jit(solution)/shard_map/all_to_all | solution.py:188
  195.3 1.2 gather_fusion.1
  196.8 0.7 multiply_reduce_fusion.2
  197.5 0.7 add_convert_fusion.1
  (63 shorter events, 3.1 us)
Async XLA Ops:
  6.5 141.4 %copy-start = (bf16[1,512,2048]{2,1,0:T(8,128)(2,1)S(1)}, bf16[1,512,2048]{2,1,0:T(8,128)(2,1)}, u32[]{:S(2)}) copy-start(bf16[1,512,2048]{2,1,0:T(8,128)(2,1)} %param.27) | copy-start | bytes 6291460
  6.5 98.8 %all-reduce.2.cloned.1.call-start = ((), (), s32[]{:S(2)}) async-start(), calls=%async_computation.3 | async-start | bytes 1048576 | tf_op jit(solution)/shard_map/psum | solution.py:143
  41.1 1.4 copy-start.1
  43.8 29.1 %copy-start.2 = (bf16[512,2048]{1,0:T(8,128)(2,1)S(1)}, bf16[512,2048]{1,0:T(8,128)(2,1)}, u32[]{:S(2)}) copy-start(bf16[512,2048]{1,0:T(8,128)(2,1)} %param.21) | copy-start | bytes 6291460
  72.9 1.4 copy-start.5
  72.9 32.5 %copy-start.3 = (bf16[128,2048]{1,0:T(8,128)(2,1)S(1)}, bf16[128,2048]{1,0:T(8,128)(2,1)}, u32[]{:S(2)}) copy-start(bf16[128,2048]{1,0:T(8,128)(2,1)} %param.14) | copy-start | bytes 1572868
  74.2 69.4 %all-gather.2.cloned.1.call-start = ((), (), s32[]{:S(2)}) async-start(), calls=%async_computation.4 | async-start | bytes 1966080 | tf_op jit(solution)/shard_map/all_gather | solution.py:177
  125.6 52.6 %reduce-scatter.2.cloned.1.call-start = ((), (), s32[]{:S(2)}) async-start(), calls=%async_computation.5 | async-start | bytes 1966080 | tf_op jit(solution)/shard_map/reduce_scatter | solution.py:185
  143.7 3.2 %copy-start.6 = (bf16[1,2048,512]{2,1,0:T(8,128)(2,1)S(1)}, bf16[1,2048,512]{2,1,0:T(8,128)(2,1)}, u32[]{:S(2)}) copy-start(bf16[1,2048,512]{2,1,0:T(8,128)(2,1)} %param.26) | copy-start | bytes 6291460
  143.7 3.2 %copy-start.7 = (bf16[8,48,2048]{2,1,0:T(8,128)(2,1)S(1)}, bf16[8,48,2048]{2,1,0:T(8,128)(2,1)}, u32[]{:S(2)}) copy-start(bf16[8,48,2048]{2,1,0:T(8,128)(2,1)} %all-gather.2.cloned.1.call-done) | copy-start | bytes 4718596
  150.0 33.7 %copy-start.4 = (f32[128,2]{0,1:T(2,128)S(1)}, f32[128,2]{0,1:T(2,128)}, u32[]{:S(2)}) copy-start(f32[128,2]{0,1:T(2,128)} %param.23) | copy-start | bytes 3076
  178.2 17.1 %all-to-all-start.1 = ((bf16[8,48,512]{2,1,0:T(8,128)(2,1)}), bf16[8,48,512]{2,1,0:T(8,128)(2,1)S(1)}, u32[]{:S(2)}, u32[]{:S(2)}) async-start(bf16[8,48,512]{2,1,0:T(8,128)(2,1)} %reduce-scatter.2.cloned.1.call-done), calls=%async_computation.2 | async-start | bytes 786432 | tf_op jit(solution)/shard_map/all_to_all | solution.py:188
Sparse Core Ops, SparseCore 0:
  74.3 30.9 all-reduce.1
  125.8 17.8 all-gather.1
  150.2 27.9 reduce-scatter.1
where the time goes:
time: 205 us
  waiting for transfers between devices  83.3 us (41%)
  blocking collectives  71.7 us (35%)
  between operations  13.5 us (7%)
  local copies, waits for them, and re-layouts  12.6 us (6%)
  matrix products  10.4 us (5%)
  other arithmetic  7.66 us (4%)
  starting transfers between devices  5.57 us (3%)
    all_gather x1, blocking collectives, shards(): key_piece = lax.all_gather(key_turned, 'sp', axis=0, tiled=True)  28.3 us
    reduce_scatter x1, waiting for transfers between devices, shards(): lax.psum_scatter(expert_part.astype(jnp.bfloat16), 'tp', scatter_dimensio...  28.1 us
    all_gather x1, blocking collectives, shards(): value_piece = lax.all_gather(value_cols, 'sp', axis=0, tiled=True)  26.8 us
    psum x1, waiting for transfers between devices, shards(): attended = lax.psum(partial_sum.astype(jnp.bfloat16), 'tp')  25.8 us
    all_gather x1, waiting for transfers between devices, shards(): feature_piece = lax.all_gather(arrived, 'tp', axis=2, tiled=True)  18 us
    all_to_all x1, blocking collectives, shards(): lax.all_to_all(outgoing, 'sp', split_axis=0, concat_axis=0, tiled=True)  16.5 us
    all_to_all x1, waiting for transfers between devices, shards(): lax.all_to_all(expert_share, 'sp', split_axis=0, concat_axis=0, tiled=True)  11.4 us
    all_to_all x1, starting transfers between devices, shards(): lax.all_to_all(expert_share, 'sp', split_axis=0, concat_axis=0, tiled=True)  5.48 us
  transfers between devices with their start and end apart: 4, of which 4 were waited for; matrix products, arithmetic and copies ran while one was open for 3% of the time, Pallas kernels for 0%

commit v1 on v0

v1 whole, which is shorter than its diff:
```python
import functools
import math

import jax
import jax.numpy as jnp
from jax import lax
from jax.experimental import pallas as pl
from jax.experimental.pallas import tpu as pltpu
from jax.sharding import PartitionSpec as P

CHANNEL_WIDTH = 128
GROUP = 4
GRID_W = 64
CORES = 2
EPSILON = 1e-06
MESH = pl.DeviceIdType.MESH
BF = jnp.bfloat16
F32 = jnp.float32


def turn_tables(positions):
    quarter = CHANNEL_WIDTH // 4
    frequency = 10000.0 ** (-jnp.arange(quarter, dtype=F32) / quarter)
    rows = (positions // GRID_W).astype(F32)[:, None] * frequency[None, :]
    cols = (positions % GRID_W).astype(F32)[:, None] * frequency[None, :]
    angles = jnp.concatenate([rows, rows, cols, cols], axis=1)
    cosine = jnp.cos(angles)
    sine = jnp.sin(angles)
    lane = jnp.arange(CHANNEL_WIDTH) // quarter
    first = (lane % 2 == 0)[None, :]
    return cosine, jnp.where(first, -sine, 0.0), jnp.where(first, 0.0, sine)


def norm_turn(x, gain, cosine, sine_a, sine_b):
    x = x.astype(F32)
    y = x * lax.rsqrt(jnp.mean(x * x, axis=-1, keepdims=True) + EPSILON) * gain
    quarter = CHANNEL_WIDTH // 4
    out = (
        y * cosine
        + pltpu.roll(y, CHANNEL_WIDTH - quarter, 1) * sine_a
        + pltpu.roll(y, quarter, 1) * sine_b
    )
    return out.astype(BF)


def dot(a, b):
    return jnp.dot(a, b, preferred_element_type=F32)


def layer_kernel(
    dims,
    skip_ref, q_ref, k_ref, v_ref, qg_ref, kg_ref, soft_ref, cos_ref, sa_ref, sb_ref,
    gain_ref, route_ref, ids_ref, wo_hbm, wg_hbm, wu_hbm, wd_hbm,
    out_ref,
    kk, vv, qs, sc, attn, pt, pk,
    p_send, p_recv, p_own, py_send, py_recv, mid,
    disp, xg, xn, r_send, r_recv, r_own, ry_send, ry_recv, ret, back,
    wo, wg, wu, wd,
    w_sem, k_s, k_r, v_s, v_r, pa_s, pa_r, py_s, py_r, d_s, d_r,
    gp_s, gp_r, gy_s, gy_r, gf_s, gf_r, rp_s, rp_r, ry_s, ry_r, b_s, b_r,
):
    n, m, tok, width, share, heads, lkv, capp, nch = dims
    A = m // CORES
    CW = CHANNEL_WIDTH
    me = lax.axis_index("sp")
    t = lax.axis_index("tp")
    a_pos = t // CORES
    core = t % CORES
    other = 1 - core
    partner = (me, a_pos * CORES + other)
    G = n // nch
    R = G * capp

    def sp_up(j):
        return (lax.rem(me + j, n), t)

    def sp_down(j):
        return (lax.rem(me + n - j, n), t)

    def a_at(i):
        return lax.rem(a_pos + i, A)

    def y_peer(i):
        return (me, a_at(i) * CORES + core)

    def cols_of(i, c):
        return pl.ds(pl.multiple_of((a_at(i) * CORES + c) * share, share), share)

    my_cols = pl.ds(pl.multiple_of(t * share, share), share)

    sends = []

    def remote(src, dst, ss, rs, dev):
        return pltpu.make_async_remote_copy(
            src_ref=src, dst_ref=dst, send_sem=ss, recv_sem=rs, device_id=dev, device_id_type=MESH
        )

    def go(cp):
        cp.start()
        sends.append(cp)
        return cp

    loads = [
        pltpu.make_async_copy(wo_hbm, wo, w_sem.at[0]),
        pltpu.make_async_copy(wg_hbm.at[0], wg, w_sem.at[1]),
        pltpu.make_async_copy(wu_hbm.at[0], wu, w_sem.at[2]),
        pltpu.make_async_copy(wd_hbm.at[0], wd, w_sem.at[3]),
    ]
    for cp in loads:
        cp.start()

    barrier = pltpu.get_barrier_semaphore()
    peers = [sp_up(j) for j in range(1, n)] + [partner] + [y_peer(i) for i in range(1, A)]
    for dev in peers:
        pl.semaphore_signal(barrier, inc=1, device_id=dev, device_id_type=MESH)

    first = (t * heads) // GROUP
    kv_cols = pl.ds(pl.multiple_of(first * CW, CW), lkv * CW)
    cosine, sine_a, sine_b = cos_ref[...], sa_ref[...], sb_ref[...]
    k_in = k_ref[:, kv_cols]
    for h in range(lkv):
        kk[0, :, h * CW:(h + 1) * CW] = norm_turn(
            k_in[:, h * CW:(h + 1) * CW], kg_ref[...], cosine, sine_a, sine_b
        )
    vv[0] = v_ref[:, kv_cols]
    pl.semaphore_wait(barrier, len(peers))
    k_cp, v_cp = {}, {}
    for j in range(1, n):
        k_cp[j] = go(remote(kk.at[0], kk.at[j], k_s.at[j], k_r.at[j], sp_up(j)))
    for j in range(1, n):
        v_cp[j] = go(remote(vv.at[0], vv.at[j], v_s.at[j], v_r.at[j], sp_up(j)))

    for h in range(heads):
        qs[h] = norm_turn(q_ref[:, h * CW:(h + 1) * CW], qg_ref[...], cosine, sine_a, sine_b)

    rel = ids_ref[...] - me
    rel = jnp.where(rel < 0, rel + n, rel)
    lanes = -(-n // 128) * 128
    lane_id = lax.broadcasted_iota(jnp.int32, (tok, lanes), 1)
    hot = [(rel[:, c:c + 1] == lane_id).astype(F32) for c in range(2)]
    lower = (
        lax.broadcasted_iota(jnp.int32, (tok, tok), 1)
        < lax.broadcasted_iota(jnp.int32, (tok, tok), 0)
    ).astype(F32)
    rank = dot(lower.astype(BF), (hot[0] + hot[1]).astype(BF))
    slot_id = lax.broadcasted_iota(jnp.int32, (tok, n * capp), 1).astype(F32)
    picks = []
    for c in range(2):
        place = rel[:, c:c + 1].astype(F32) * capp + jnp.sum(hot[c] * rank, axis=1, keepdims=True)
        picks.append((slot_id == place).astype(F32))
        pk[c] = picks[c].astype(BF)
    pt[...] = jnp.transpose(picks[0] + picks[1]).astype(BF)

    group = heads // lkv
    for j in range(n):
        if j:
            k_cp[j].wait_recv()
        for g in range(lkv):
            qg = qs[g * group:(g + 1) * group].reshape(group * tok, CW)
            s = lax.dot_general(
                qg, kk[j, :, g * CW:(g + 1) * CW], (((1,), (1,)), ((), ())),
                preferred_element_type=F32,
            )
            sc[pl.ds(g * group * tok, group * tok), j * tok:(j + 1) * tok] = s
    for j in range(1, n):
        v_cp[j].wait_recv()
    for h in range(heads):
        g = h // group
        s = sc[h * tok:(h + 1) * tok, :] * (soft_ref[h] * (1.0 / math.sqrt(CW)))
        e = jnp.exp(s - jnp.max(s, axis=-1, keepdims=True))
        total = jnp.sum(e, axis=-1, keepdims=True)
        v_all = vv[:, :, g * CW:(g + 1) * CW].reshape(n * tok, CW)
        attn[:, h * CW:(h + 1) * CW] = (dot(e.astype(BF), v_all) / total).astype(BF)

    loads[0].wait()
    att = attn[...]
    order = list(range(1, A)) + [0]
    pa_cp, py_cp = {}, {}
    for i in order:
        p_send[i] = dot(att, wo[:, cols_of(i, other)]).astype(BF)
        pa_cp[i] = go(remote(p_send.at[i], p_recv.at[i], pa_s.at[i], pa_r.at[i], partner))
    for i in order:
        p_own[i] = dot(att, wo[:, cols_of(i, core)])
    for i in range(1, A):
        pa_cp[i].wait_recv()
        py_send[i] = (p_own[i] + p_recv[i].astype(F32)).astype(BF)
        py_cp[i] = go(remote(py_send.at[i], py_recv.at[i], py_s.at[i], py_r.at[i], y_peer(i)))
    pa_cp[0].wait_recv()
    acc = p_own[0] + p_recv[0].astype(F32)
    for i in range(1, A):
        py_cp[i].wait_recv()
        acc = acc + py_recv[i].astype(F32)
    mid[...] = (skip_ref[:, my_cols].astype(F32) + acc.astype(BF).astype(F32)).astype(BF)

    disp[...] = dot(pt[...], mid[...]).astype(BF)
    d_cp = {}
    for j in range(1, n):
        d_cp[j] = go(remote(
            disp.at[pl.ds(j * capp, capp)], xg.at[pl.ds(j * capp, capp), my_cols],
            d_s.at[j], d_r.at[j], sp_up(j),
        ))
    xg[pl.ds(0, capp), my_cols] = disp[pl.ds(0, capp), :]

    gp_cp, gy_cp, gf_cp = {}, {}, {}
    for ch in range(nch):
        rows = pl.ds(ch * R, R)
        for j in range(ch * G, (ch + 1) * G):
            if j:
                d_cp[j].wait_recv()
        mine = xg.at[rows, my_cols]
        for i in range(1, A):
            gy_cp[ch, i] = go(remote(mine, mine, gy_s.at[ch, i], gy_r.at[ch, i], y_peer(i)))
        gp_cp[ch] = go(remote(mine, mine, gp_s.at[ch], gp_r.at[ch], partner))
    for ch in range(nch):
        rows = pl.ds(ch * R, R)
        for i in range(1, A):
            gy_cp[ch, i].wait_recv()
            piece = xg.at[rows, cols_of(A - i, core)]
            gf_cp[ch, i] = go(remote(piece, piece, gf_s.at[ch, i], gf_r.at[ch, i], partner))
    rp_cp, ry_cp = {}, {}
    for ch in range(nch):
        rows = pl.ds(ch * R, R)
        gp_cp[ch].wait_recv()
        for i in range(1, A):
            gf_cp[ch, i].wait_recv()
        x = xg[rows, :].astype(F32)
        xn[...] = (
            x * lax.rsqrt(jnp.mean(x * x, axis=-1, keepdims=True) + EPSILON) * gain_ref[...]
        ).astype(BF)
        if ch == 0:
            loads[1].wait()
            loads[2].wait()
        x = xn[...]
        gate = dot(x, wg[...])
        up = dot(x, wu[...])
        hidden = (gate / (1.0 + jnp.exp(-gate)) * up).astype(BF)
        if ch == 0:
            loads[3].wait()
        for i in order:
            r_send[ch, i] = dot(hidden, wd[:, cols_of(i, other)]).astype(BF)
            rp_cp[ch, i] = go(remote(
                r_send.at[ch, i], r_recv.at[ch, i], rp_s.at[ch, i], rp_r.at[ch, i], partner
            ))
        for i in order:
            r_own[ch, i] = dot(hidden, wd[:, cols_of(i, core)])
        for i in range(1, A):
            rp_cp[ch, i].wait_recv()
            ry_send[ch, i] = (r_own[ch, i] + r_recv[ch, i].astype(F32)).astype(BF)
            ry_cp[ch, i] = go(remote(
                ry_send.at[ch, i], ry_recv.at[ch, i], ry_s.at[ch, i], ry_r.at[ch, i], y_peer(i)
            ))
    b_cp = {}
    for ch in range(nch):
        rp_cp[ch, 0].wait_recv()
        acc = r_own[ch, 0] + r_recv[ch, 0].astype(F32)
        for i in range(1, A):
            ry_cp[ch, i].wait_recv()
            acc = acc + ry_recv[ch, i].astype(F32)
        ret[pl.ds(ch * R, R), :] = acc.astype(BF)
        for j in range(ch * G, (ch + 1) * G):
            rows = pl.ds(j * capp, capp)
            if j:
                b_cp[j] = go(remote(ret.at[rows], back.at[rows], b_s.at[j], b_r.at[j], sp_down(j)))
            else:
                back[rows, :] = ret[rows, :]

    route = route_ref[...]
    top = jnp.max(route, axis=1, keepdims=True)
    e = jnp.exp(route - top)
    weight = e / jnp.sum(e, axis=1, keepdims=True)
    for j in range(1, n):
        b_cp[j].wait_recv()
    got = back[...]
    out = weight[:, 0:1] * dot(pk[0], got) + weight[:, 1:2] * dot(pk[1], got)
    out_ref[...] = (mid[...].astype(F32) + out).astype(BF)
    for cp in sends:
        cp.wait_send()


def shards(
    skip, q, k, v, q_gain, k_gain, soft, mix, gain, route, ids, w_gate, w_up, w_down
):
    n, m = lax.axis_size("sp"), lax.axis_size("tp")
    tok, width = skip.shape
    share = width // m
    heads = q.shape[1] // CHANNEL_WIDTH
    lkv = max(1, heads // GROUP)
    cap = max(2, 3 * tok * ids.shape[1] // (2 * n))
    capp = -(-cap // 16) * 16
    nch = 2
    A = m // CORES
    eff = w_gate.shape[2]
    rows_all = n * capp
    R = rows_all // nch
    kvw = lkv * CHANNEL_WIDTH
    positions = lax.axis_index("sp") * tok + jnp.arange(tok, dtype=jnp.int32)
    cosine, sine_a, sine_b = turn_tables(positions)
    vm = pl.BlockSpec(memory_space=pltpu.VMEM)
    hbm = pl.BlockSpec(memory_space=pl.ANY)
    dma = pltpu.SemaphoreType.DMA
    dims = (n, m, tok, width, share, heads, lkv, capp, nch)
    pair = (nch, A)
    call = pl.pallas_call(
        functools.partial(layer_kernel, dims),
        out_shape=jax.ShapeDtypeStruct((tok, share), BF),
        in_specs=[vm] * 6 + [pl.BlockSpec(memory_space=pltpu.SMEM)] + [vm] * 6 + [hbm] * 4,
        out_specs=vm,
        scratch_shapes=[
            pltpu.VMEM((n, tok, kvw), BF),
            pltpu.VMEM((n, tok, kvw), BF),
            pltpu.VMEM((heads, tok, CHANNEL_WIDTH), BF),
            pltpu.VMEM((heads * tok, n * tok), F32),
            pltpu.VMEM((tok, heads * CHANNEL_WIDTH), BF),
            pltpu.VMEM((rows_all, tok), BF),
            pltpu.VMEM((2, tok, rows_all), BF),
            pltpu.VMEM((A, tok, share), BF),
            pltpu.VMEM((A, tok, share), BF),
            pltpu.VMEM((A, tok, share), F32),
            pltpu.VMEM((A, tok, share), BF),
            pltpu.VMEM((A, tok, share), BF),
            pltpu.VMEM((tok, share), BF),
            pltpu.VMEM((rows_all, share), BF),
            pltpu.VMEM((rows_all, width), BF),
            pltpu.VMEM((R, width), BF),
            pltpu.VMEM(pair + (R, share), BF),
            pltpu.VMEM(pair + (R, share), BF),
            pltpu.VMEM(pair + (R, share), F32),
            pltpu.VMEM(pair + (R, share), BF),
            pltpu.VMEM(pair + (R, share), BF),
            pltpu.VMEM((rows_all, share), BF),
            pltpu.VMEM((rows_all, share), BF),
            pltpu.VMEM(mix.shape, BF),
            pltpu.VMEM(w_gate.shape[1:], BF),
            pltpu.VMEM(w_up.shape[1:], BF),
            pltpu.VMEM(w_down.shape[1:], BF),
            dma((4,)),
            dma((n,)), dma((n,)), dma((n,)), dma((n,)),
            dma((A,)), dma((A,)), dma((A,)), dma((A,)),
            dma((n,)), dma((n,)),
            dma((nch,)), dma((nch,)), dma(pair), dma(pair), dma(pair), dma(pair),
            dma(pair), dma(pair), dma(pair), dma(pair),
            dma((n,)), dma((n,)),
        ],
        compiler_params=pltpu.CompilerParams(
            collective_id=0, has_side_effects=True, vmem_limit_bytes=56 * 1024 * 1024
        ),
    )
    return call(
        skip, q, k, v, q_gain.reshape(1, -1), k_gain.reshape(1, -1), soft,
        cosine, sine_a, sine_b, gain.reshape(1, -1), route, ids, mix, w_gate, w_up, w_down,
    )


def solution(mesh):
    in_specs = (
        P("sp", None),
        P("sp", "tp"),
        P("sp", None),
        P("sp", None),
        P(),
        P(),
        P("tp"),
        P("tp", None),
        P(),
        P("sp", None),
        P("sp", None),
        P("sp", None, "tp"),
        P("sp", None, "tp"),
        P("sp", "tp", None),
    )
    out_specs = P("sp", "tp")
    return jax.shard_map(shards, mesh=mesh, in_specs=in_specs, out_specs=out_specs, check_vma=False)
```

time: 205 us -> 74.3 us (0.36)
  waiting for transfers between devices: 83.3 us -> 0 us
  blocking collectives: 71.7 us -> 0 us
  Pallas kernels: 0 us -> 68.5 us
  between operations: 13.5 us -> 0.03 us
  matrix products: 10.4 us -> 0 us
  local copies, waits for them, and re-layouts: 12.6 us -> 4.39 us
  other arithmetic: 7.66 us -> 1.14 us
  starting transfers between devices: 5.57 us -> 0 us
    pallas_call x0 -> x1, Pallas kernels: none -> 68.5 us  [shards(): call(skip, q, k, v, q_gain.reshape(1, -1), k_gain.reshape(1, -1), soft, c...]
    all_gather x2 -> x0, blocking collectives: 55.2 us -> none  [the longest x1 28.3 us: shards(): key_piece = lax.all_gather(key_turned, 'sp', axis=0, tiled=True)]
    reduce_scatter x1 -> x0, waiting for transfers between devices: 28.1 us -> none  [shards(): lax.psum_scatter(expert_part.astype(jnp.bfloat16), 'tp', scatter_dimensio...]
    psum x1 -> x0, waiting for transfers between devices: 25.8 us -> none  [shards(): attended = lax.psum(partial_sum.astype(jnp.bfloat16), 'tp')]
    all_gather x1 -> x0, waiting for transfers between devices: 18 us -> none  [shards(): feature_piece = lax.all_gather(arrived, 'tp', axis=2, tiled=True)]
    all_to_all x1 -> x0, blocking collectives: 16.5 us -> none  [shards(): lax.all_to_all(outgoing, 'sp', split_axis=0, concat_axis=0, tiled=True)]
    all_to_all x1 -> x0, waiting for transfers between devices: 11.4 us -> none  [shards(): lax.all_to_all(expert_share, 'sp', split_axis=0, concat_axis=0, tiled=True)]
    dot_general x6 -> x0, matrix products: 10.4 us -> none  [the longest x1 3.18 us: shards(): jnp.dot(flat_piece, gate_local, preferred_element_type=jnp.float32)]
  transfers between devices with their start and end apart: 4 -> 0, of which waited for: 4 -> 0; matrix products, arithmetic and copies ran while one was open for 3% -> 0% of each run, Pallas kernels for 0% -> 0%
where the time goes in v1:
time: 74.3 us; the launch traced here: 74.1 us
  Pallas kernels  68.5 us (92%)
  local copies, waits for them, and re-layouts  4.39 us (6%)
  other arithmetic  1.14 us (2%)
    pallas_call x1, Pallas kernels, shards(): call(skip, q, k, v, q_gain.reshape(1, -1), k_gain.reshape(1, -1), soft, c...  68.5 us
    unnamed x3, local copies, waits for them, and re-layouts  4.39 us

profile of v1, /device:TPU:0, one launch (start us, length us, event | category | flops | bytes accessed | tf_op | source)
XLA Modules:
  0.0 74.1 jit_solution(6819942052795565232)
XLA Ops:
  0.0 0.1 broadcast_multiply_fusion.1
  0.1 1.0 %broadcast_select_fusion = (f32[128,128]{1,0:T(8,128)}, f32[128,128]{1,0:T(8,128)}, f32[128,128]{1,0:T(8,128)}) fusion(pred[128]{0:T(512)(128)(4,1)S(1)} %fusion.3, f32[128,32]{1,0:T(8,128)S(1)} %get-tuple-element.9, f32[128,32]{1,0:T(8,128)S(1)} %get-tuple-element.8), kind=kLoop, calls=%fused_computation.2 | loop fusion | flops 98304 | bytes 229504 | tf_op jit(solution)/shard_map/jit(_where)/select_n | solution.py:31
  1.2 1.4 %copy.15.route_ref = f32[128,2]{1,0:T(8,128)} copy(f32[128,2]{0,1:T(2,128)} %param.23) | data formatting | bytes 2048 | tf_op args[9]
  2.6 1.4 %copy.16.ids_ref = s32[128,2]{1,0:T(8,128)} copy(s32[128,2]{0,1:T(2,128)} %param.24) | data formatting | bytes 2048 | tf_op args[10]
  4.0 68.5 %shard_map.136 = bf16[128,512]{1,0:T(8,128)(2,1)} custom-call(bf16[128,2048]{1,0:T(8,128)(2,1)} %skip_ref.1, bf16[128,512]{1,0:T(8,128)(2,1)} %q_ref.1, bf16[128,512]{1,0:T(8,128)(2,1)} %k_ref.1, bf16[128,512]{1,0:T(8,128)(2,1)} %v_ref.1, f32[1,128]{1,0:T(1,128)} %bitcast.4, f32[1,128]{1,0:T(1,128)} %bitcast.5, f32[4]{0:T(128)} %soft_ref.1, ...), custom_call_target="tpu_custom_call" | custom-call | tf_op jit(solution)/shard_map/pallas_call | solution.py:348
  72.5 1.6 %copy.18 = bf16[128,512]{1,0:T(8,128)(2,1)} copy(bf16[128,512]{1,0:T(8,128)(2,1)} %shard_map.136) | data formatting | bytes 262144
  (3 shorter events, 0.0 us)

commit v2 on v1

--- a/solution.py
+++ b/solution.py
@@ -133,11 +133,19 @@
     for h in range(heads):
         qs[h] = norm_turn(q_ref[:, h * CW:(h + 1) * CW], qg_ref[...], cosine, sine_a, sine_b)
 
+    def column(row):
+        return jnp.transpose(jnp.broadcast_to(row, (tok, tok)))[:, 0:1]
+
     rel = ids_ref[...] - me
-    rel = jnp.where(rel < 0, rel + n, rel)
+    rel = jnp.where(rel < 0, rel + n, rel).astype(F32)
+    rel = [column(rel[c:c + 1, :]) for c in range(2)]
+    route = [column(route_ref[c:c + 1, :]) for c in range(2)]
+    top = jnp.maximum(route[0], route[1])
+    e0, e1 = jnp.exp(route[0] - top), jnp.exp(route[1] - top)
+    weight = [e0 / (e0 + e1), e1 / (e0 + e1)]
     lanes = -(-n // 128) * 128
-    lane_id = lax.broadcasted_iota(jnp.int32, (tok, lanes), 1)
-    hot = [(rel[:, c:c + 1] == lane_id).astype(F32) for c in range(2)]
+    lane_id = lax.broadcasted_iota(jnp.int32, (tok, lanes), 1).astype(F32)
+    hot = [(rel[c] == lane_id).astype(F32) for c in range(2)]
     lower = (
         lax.broadcasted_iota(jnp.int32, (tok, tok), 1)
         < lax.broadcasted_iota(jnp.int32, (tok, tok), 0)
@@ -146,7 +154,7 @@
     slot_id = lax.broadcasted_iota(jnp.int32, (tok, n * capp), 1).astype(F32)
     picks = []
     for c in range(2):
-        place = rel[:, c:c + 1].astype(F32) * capp + jnp.sum(hot[c] * rank, axis=1, keepdims=True)
+        place = rel[c] * capp + jnp.sum(hot[c] * rank, axis=1, keepdims=True)
         picks.append((slot_id == place).astype(F32))
         pk[c] = picks[c].astype(BF)
     pt[...] = jnp.transpose(picks[0] + picks[1]).astype(BF)
@@ -201,24 +209,24 @@
         ))
     xg[pl.ds(0, capp), my_cols] = disp[pl.ds(0, capp), :]
 
-    gp_cp, gy_cp, gf_cp = {}, {}, {}
-    for ch in range(nch):
-        rows = pl.ds(ch * R, R)
+    gp_cp, gy_cp, gf_cp, rp_cp, ry_cp, b_cp = {}, {}, {}, {}, {}, {}
+
+    def spread(ch):
         for j in range(ch * G, (ch + 1) * G):
             if j:
                 d_cp[j].wait_recv()
-        mine = xg.at[rows, my_cols]
+        mine = xg.at[pl.ds(ch * R, R), my_cols]
         for i in range(1, A):
             gy_cp[ch, i] = go(remote(mine, mine, gy_s.at[ch, i], gy_r.at[ch, i], y_peer(i)))
         gp_cp[ch] = go(remote(mine, mine, gp_s.at[ch], gp_r.at[ch], partner))
-    for ch in range(nch):
-        rows = pl.ds(ch * R, R)
+
+    def forward(ch):
         for i in range(1, A):
             gy_cp[ch, i].wait_recv()
-            piece = xg.at[rows, cols_of(A - i, core)]
+            piece = xg.at[pl.ds(ch * R, R), cols_of(A - i, core)]
             gf_cp[ch, i] = go(remote(piece, piece, gf_s.at[ch, i], gf_r.at[ch, i], partner))
-    rp_cp, ry_cp = {}, {}
-    for ch in range(nch):
+
+    def serve(ch):
         rows = pl.ds(ch * R, R)
         gp_cp[ch].wait_recv()
         for i in range(1, A):
@@ -243,14 +251,16 @@
             ))
         for i in order:
             r_own[ch, i] = dot(hidden, wd[:, cols_of(i, core)])
+
+    def join(ch):
         for i in range(1, A):
             rp_cp[ch, i].wait_recv()
             ry_send[ch, i] = (r_own[ch, i] + r_recv[ch, i].astype(F32)).astype(BF)
             ry_cp[ch, i] = go(remote(
                 ry_send.at[ch, i], ry_recv.at[ch, i], ry_s.at[ch, i], ry_r.at[ch, i], y_peer(i)
             ))
-    b_cp = {}
-    for ch in range(nch):
+
+    def give_back(ch):
         rp_cp[ch, 0].wait_recv()
         acc = r_own[ch, 0] + r_recv[ch, 0].astype(F32)
         for i in range(1, A):
@@ -264,14 +274,16 @@
             else:
                 back[rows, :] = ret[rows, :]
 
-    route = route_ref[...]
-    top = jnp.max(route, axis=1, keepdims=True)
-    e = jnp.exp(route - top)
-    weight = e / jnp.sum(e, axis=1, keepdims=True)
+    stages = (spread, forward, serve, join, give_back)
+    for step in range(nch + len(stages) - 1):
+        for late, stage in enumerate(stages):
+            if 0 <= step - late < nch:
+                stage(step - late)
+
     for j in range(1, n):
         b_cp[j].wait_recv()
     got = back[...]
-    out = weight[:, 0:1] * dot(pk[0], got) + weight[:, 1:2] * dot(pk[1], got)
+    out = weight[0] * dot(pk[0], got) + weight[1] * dot(pk[1], got)
     out_ref[...] = (mid[...].astype(F32) + out).astype(BF)
     for cp in sends:
         cp.wait_send()
@@ -287,7 +299,7 @@
     lkv = max(1, heads // GROUP)
     cap = max(2, 3 * tok * ids.shape[1] // (2 * n))
     capp = -(-cap // 16) * 16
-    nch = 2
+    nch = math.gcd(n, 4)
     A = m // CORES
     eff = w_gate.shape[2]
     rows_all = n * capp
@@ -347,7 +359,7 @@
     )
     return call(
         skip, q, k, v, q_gain.reshape(1, -1), k_gain.reshape(1, -1), soft,
-        cosine, sine_a, sine_b, gain.reshape(1, -1), route, ids, mix, w_gate, w_up, w_down,
+        cosine, sine_a, sine_b, gain.reshape(1, -1), route.T, ids.T, mix, w_gate, w_up, w_down,
     )
 
 

time: 74.3 us -> 66.7 us (0.90)
  Pallas kernels: 68.5 us -> 63.9 us
  local copies, waits for them, and re-layouts: 4.39 us -> 1.57 us
    pallas_call x1, Pallas kernels: 68.5 us -> 63.9 us  [shards(): call(skip, q, k, v, q_gain.reshape(1, -1), k_gain.reshape(1, -1), soft, c...]
    unnamed x3 -> x1, local copies, waits for them, and re-layouts: 4.39 us -> 1.57 us
where the time goes in v2:
time: 66.7 us; the launch traced here: 66.6 us
  Pallas kernels  63.9 us (96%)
  local copies, waits for them, and re-layouts  1.57 us (2%)
  other arithmetic  1.14 us (2%)
    pallas_call x1, Pallas kernels, shards(): call(skip, q, k, v, q_gain.reshape(1, -1), k_gain.reshape(1, -1), soft, c...  63.9 us
    unnamed x1, local copies, waits for them, and re-layouts  1.57 us

profile of v2, /device:TPU:0, one launch (start us, length us, event | category | flops | bytes accessed | tf_op | source)
XLA Modules:
  0.0 66.6 jit_solution(6424419854936240025)
XLA Ops:
  0.0 0.1 broadcast_multiply_fusion.1
  0.1 1.0 %broadcast_select_fusion = (f32[128,128]{1,0:T(8,128)}, f32[128,128]{1,0:T(8,128)}, f32[128,128]{1,0:T(8,128)}) fusion(pred[128]{0:T(512)(128)(4,1)S(1)} %fusion.3, f32[128,32]{1,0:T(8,128)S(1)} %get-tuple-element.9, f32[128,32]{1,0:T(8,128)S(1)} %get-tuple-element.8), kind=kLoop, calls=%fused_computation.2 | loop fusion | flops 98304 | bytes 229504 | tf_op jit(solution)/shard_map/jit(_where)/select_n | solution.py:31
  1.2 63.9 %shard_map.136 = bf16[128,512]{1,0:T(8,128)(2,1)} custom-call(bf16[128,2048]{1,0:T(8,128)(2,1)} %skip_ref.1, bf16[128,512]{1,0:T(8,128)(2,1)} %q_ref.1, bf16[128,512]{1,0:T(8,128)(2,1)} %k_ref.1, bf16[128,512]{1,0:T(8,128)(2,1)} %v_ref.1, f32[1,128]{1,0:T(1,128)} %bitcast.8, f32[1,128]{1,0:T(1,128)} %bitcast.9, f32[4]{0:T(128)} %soft_ref.1, ...), custom_call_target="tpu_custom_call" | custom-call | tf_op jit(solution)/shard_map/pallas_call | solution.py:360
  65.0 1.6 %copy.16 = bf16[128,512]{1,0:T(8,128)(2,1)} copy(bf16[128,512]{1,0:T(8,128)(2,1)} %shard_map.136) | data formatting | bytes 262144
  (3 shorter events, 0.0 us)

commit v3 on v2

--- a/solution.py
+++ b/solution.py
@@ -124,11 +124,22 @@
         )
     vv[0] = v_ref[:, kv_cols]
     pl.semaphore_wait(barrier, len(peers))
+    X = math.gcd(n, 2)
+    beside = (me + 1 - 2 * lax.rem(me, 2), t)
     k_cp, v_cp = {}, {}
-    for j in range(1, n):
-        k_cp[j] = go(remote(kk.at[0], kk.at[j], k_s.at[j], k_r.at[j], sp_up(j)))
-    for j in range(1, n):
-        v_cp[j] = go(remote(vv.at[0], vv.at[j], v_s.at[j], v_r.at[j], sp_up(j)))
+
+    def to_below(cps, buf, ss, rs):
+        for j in range(X, n, X):
+            cps[j] = go(remote(buf.at[0], buf.at[j], ss.at[j], rs.at[j], sp_up(j)))
+
+    def to_side(cps, buf, ss, rs, j):
+        if X > 1:
+            cps[j + 1] = go(remote(buf.at[j], buf.at[j + 1], ss.at[j + 1], rs.at[j + 1], beside))
+
+    to_below(k_cp, kk, k_s, k_r)
+    to_side(k_cp, kk, k_s, k_r, 0)
+    to_below(v_cp, vv, v_s, v_r)
+    to_side(v_cp, vv, v_s, v_r, 0)
 
     for h in range(heads):
         qs[h] = norm_turn(q_ref[:, h * CW:(h + 1) * CW], qg_ref[...], cosine, sine_a, sine_b)
@@ -160,9 +171,8 @@
     pt[...] = jnp.transpose(picks[0] + picks[1]).astype(BF)
 
     group = heads // lkv
-    for j in range(n):
-        if j:
-            k_cp[j].wait_recv()
+
+    def score(j):
         for g in range(lkv):
             qg = qs[g * group:(g + 1) * group].reshape(group * tok, CW)
             s = lax.dot_general(
@@ -170,8 +180,23 @@
                 preferred_element_type=F32,
             )
             sc[pl.ds(g * group * tok, group * tok), j * tok:(j + 1) * tok] = s
-    for j in range(1, n):
+
+    for j in range(X, n, X):
+        k_cp[j].wait_recv()
+        to_side(k_cp, kk, k_s, k_r, j)
+        if j == X:
+            score(0)
+        score(j)
+    for j in range(X, n, X):
         v_cp[j].wait_recv()
+        to_side(v_cp, vv, v_s, v_r, j)
+    for j in range(0, n, X):
+        for side in range(1, X):
+            k_cp[j + side].wait_recv()
+            score(j + side)
+    for j in range(0, n, X):
+        for side in range(1, X):
+            v_cp[j + side].wait_recv()
     for h in range(heads):
         g = h // group
         s = sc[h * tok:(h + 1) * tok, :] * (soft_ref[h] * (1.0 / math.sqrt(CW)))

time: 66.7 us -> 63.3 us (0.949)
  Pallas kernels: 63.9 us -> 60.4 us
    pallas_call x1, Pallas kernels: 63.9 us -> 60.4 us  [shards(): call(skip, q, k, v, q_gain.reshape(1, -1), k_gain.reshape(1, -1), soft, c...]
where the time goes in v3:
time: 63.3 us; the launch traced here: 63.2 us
  Pallas kernels  60.4 us (95%)
  local copies, waits for them, and re-layouts  1.57 us (2%)
  other arithmetic  1.14 us (2%)
    pallas_call x1, Pallas kernels, shards(): call(skip, q, k, v, q_gain.reshape(1, -1), k_gain.reshape(1, -1), soft, c...  60.4 us
    unnamed x1, local copies, waits for them, and re-layouts  1.57 us

profile of v3, /device:TPU:0, one launch (start us, length us, event | category | flops | bytes accessed | tf_op | source)
XLA Modules:
  0.0 63.2 jit_solution(9299738652658483763)
XLA Ops:
  0.0 0.1 broadcast_multiply_fusion.1
  0.1 1.0 %broadcast_select_fusion = (f32[128,128]{1,0:T(8,128)}, f32[128,128]{1,0:T(8,128)}, f32[128,128]{1,0:T(8,128)}) fusion(pred[128]{0:T(512)(128)(4,1)S(1)} %fusion.3, f32[128,32]{1,0:T(8,128)S(1)} %get-tuple-element.9, f32[128,32]{1,0:T(8,128)S(1)} %get-tuple-element.8), kind=kLoop, calls=%fused_computation.2 | loop fusion | flops 98304 | bytes 229504 | tf_op jit(solution)/shard_map/jit(_where)/select_n | solution.py:31
  1.2 60.4 %shard_map.136 = bf16[128,512]{1,0:T(8,128)(2,1)} custom-call(bf16[128,2048]{1,0:T(8,128)(2,1)} %skip_ref.1, bf16[128,512]{1,0:T(8,128)(2,1)} %q_ref.1, bf16[128,512]{1,0:T(8,128)(2,1)} %k_ref.1, bf16[128,512]{1,0:T(8,128)(2,1)} %v_ref.1, f32[1,128]{1,0:T(1,128)} %bitcast.8, f32[1,128]{1,0:T(1,128)} %bitcast.9, f32[4]{0:T(128)} %soft_ref.1, ...), custom_call_target="tpu_custom_call" | custom-call | tf_op jit(solution)/shard_map/pallas_call | solution.py:385
  61.6 1.6 %copy.16 = bf16[128,512]{1,0:T(8,128)(2,1)} copy(bf16[128,512]{1,0:T(8,128)(2,1)} %shard_map.136) | data formatting | bytes 262144
  (3 shorter events, 0.0 us)
